TPU v7x, 32 devices: a whole 2x2x4 slice. The times are simulated.
32 devices in a mesh: sp: 8 (over z, y), tp: 4 (over x, core).
Axes of the slice: x: 2, y: 2, z: 4, core: 2. Of those that a mesh axis runs over, the one named last changes fastest.
Arguments:
- tokens: bfloat16 [2048, 2048], P('sp', 'tp'), may hold values from -6 to 6
- in_gain: float32 [2048], replicated, may hold values from 0.1 to 1.9
- query_down: bfloat16 [2048, 512], replicated, may hold values from -0.125 to 0.125
- latent_down: bfloat16 [2048, 256], replicated, may hold values from -0.125 to 0.125
- rope_down: bfloat16 [2048, 32], replicated, may hold values from -0.125 to 0.125
- query_gain: float32 [512], replicated, may hold values from 0.5 to 12
- latent_gain: float32 [256], replicated, may hold values from 0.5 to 12
- query_nope: bfloat16 [512, 1024], P(None, 'tp'), may hold values from -0.25 to 0.25
- query_rope: bfloat16 [512, 512], P(None, 'tp'), may hold values from -0.25 to 0.25
- key_up: bfloat16 [256, 1024], P(None, 'tp'), may hold values from -0.375 to 0.375
- value_up: bfloat16 [256, 1024], P(None, 'tp'), may hold values from -0.375 to 0.375
- conv_value: bfloat16 [2048, 2048], P(None, 'tp'), may hold values from -0.125 to 0.125
- conv_gate: bfloat16 [2048, 2048], P(None, 'tp'), may hold values from -0.125 to 0.125
- conv_taps: float32 [31, 2048], P(None, 'tp'), may hold values from -1 to 1
- conv_bias: float32 [2048], P('tp'), may hold values from 0.05 to 2.25
- channel_gain: float32 [2048], P('tp'), may hold values from 0.1 to 1.9
- out_attend: bfloat16 [1024, 2048], P('tp'), may hold values from -0.109375 to 0.109375
- out_conv: bfloat16 [2048, 2048], P('tp'), may hold values from -0.109375 to 0.109375
Outputs:
- mixed: bfloat16 [2048, 2048], P('sp', 'tp')
All inputs are finite; a program needn't handle non-finite values.
Results may differ from a plain program's by a relative error of at most 0.013.
The roundings to bfloat16 on the way count: a program that leaves them out, or rounds other values in their place, can miss the bound.
Values may be sent and summed in bfloat16 or wider, within the bound.
A program may use at most 128 MiB of HBM per device.

v0:
```python
import math
import jax
import jax.numpy as jnp
from jax import lax
from jax.sharding import PartitionSpec as P

eps_norm = 1e-06
eps_layer = 1e-05
theta = 10000.0


def padded_2(cells, sides, width):
    for axis, dim in sides:
        count = lax.axis_size(axis)
        ends = count - 1
        head = lax.slice_in_dim(cells, 0, width, axis=dim)
        tail = lax.slice_in_dim(cells, cells.shape[dim] - width, cells.shape[dim], axis=dim)
        cells = jnp.concatenate(
            [
                lax.ppermute(tail, axis, [(i, (i + 1) % count) for i in range(ends)]),
                cells,
                lax.ppermute(head, axis, [((i + 1) % count, i) for i in range(ends)]),
            ],
            axis=dim,
        )
    return cells


def rms_scale(values, gain):
    return values * lax.rsqrt(jnp.mean(values * values, axis=-1, keepdims=True) + eps_norm) * gain


def rotate(values, positions):
    half = values.shape[-1] // 2
    freqs = theta ** (-jnp.arange(half).astype(jnp.float32) / half)
    angles = positions[..., None] * freqs
    cosine = jnp.cos(angles)
    sine = jnp.sin(angles)
    first = values[..., :half]
    second = values[..., half:]
    return jnp.concatenate(
        [first * cosine - second * sine, second * cosine + first * sine], axis=-1
    )


def attend_block(state, q_heads, r_heads, k_nope, values, rope_key):
    highest, total, weighted = state
    heads = q_heads.shape[1]
    key_heads = k_nope.reshape(k_nope.shape[0], heads, -1)
    value_heads = values.reshape(values.shape[0], heads, -1)
    score_scale = (q_heads.shape[2] + r_heads.shape[2]) ** (-0.5)
    scores = (
        jnp.einsum("qhd,khd->hqk", q_heads, key_heads, preferred_element_type=jnp.float32)
        + jnp.einsum("qhd,kd->hqk", r_heads, rope_key, preferred_element_type=jnp.float32)
    ) * score_scale
    new_high = jnp.maximum(highest, jnp.max(scores, axis=-1))
    factor = jnp.exp(highest - new_high)
    weight = jnp.exp(scores - new_high[..., None])
    total = total * factor + jnp.sum(weight, axis=-1)
    weighted = weighted * factor[..., None] + jnp.einsum(
        "hqk,khd->hqd", weight.astype(jnp.bfloat16), value_heads, preferred_element_type=jnp.float32
    )
    return (new_high, total, weighted)


def over_blocks(state, arrays, step):
    count = arrays[0].shape[0]
    size = math.gcd(count, 1024)
    shaped = tuple((item.reshape((count // size, size) + item.shape[1:]) for item in arrays))

    def one_block(carry, block):
        return (step(carry, block), None)

    state, unused = lax.scan(one_block, state, shaped)
    return state


def per_device(
    tokens,
    in_gain,
    query_down,
    latent_down,
    rope_down,
    query_gain,
    latent_gain,
    query_nope,
    query_rope,
    key_up,
    value_up,
    conv_value,
    conv_gate,
    conv_taps,
    conv_bias,
    channel_gain,
    out_attend,
    out_conv,
):
    row_count = tokens.shape[0]
    width = in_gain.shape[0]
    local_ch = conv_value.shape[1]
    positions = (lax.axis_index("sp") * row_count + jnp.arange(row_count)).astype(jnp.float32)
    piece_f = lax.all_gather(tokens, "tp", axis=1, tiled=True).astype(jnp.float32)
    scaled = (piece_f * in_gain).astype(jnp.bfloat16)

    def add_rows(weight):
        return jnp.dot(scaled, weight, preferred_element_type=jnp.float32)

    square_sum = jnp.sum(piece_f * piece_f, axis=1)
    q_pre = add_rows(query_down)
    kv_pre = add_rows(latent_down)
    rope_pre = add_rows(rope_down)
    value_pre = add_rows(conv_value)
    gate_pre = add_rows(conv_gate)
    row_scale = lax.rsqrt(square_sum / width + eps_norm)[:, None]
    q_latent = rms_scale(row_scale * q_pre, query_gain).astype(jnp.bfloat16)
    kv_latent = rms_scale(row_scale * kv_pre, latent_gain).astype(jnp.bfloat16)
    rope_key = rotate(row_scale * rope_pre, positions).astype(jnp.bfloat16)
    rope_size = rope_down.shape[1]
    heads = query_rope.shape[1] // rope_size
    q_heads = (
        jnp.dot(q_latent, query_nope, preferred_element_type=jnp.float32)
        .astype(jnp.bfloat16)
        .reshape(row_count, heads, -1)
    )
    q_turn = jnp.dot(q_latent, query_rope, preferred_element_type=jnp.float32).reshape(
        row_count, heads, rope_size
    )
    r_heads = rotate(q_turn, positions[:, None]).astype(jnp.bfloat16)
    value_size = value_up.shape[1] // heads
    start_state = (
        jnp.full((heads, row_count), -jnp.inf, jnp.float32),
        jnp.zeros((heads, row_count), jnp.float32),
        jnp.zeros((heads, row_count, value_size), jnp.float32),
    )

    def latent_step(state, block):
        k_nope = jnp.dot(block[0], key_up, preferred_element_type=jnp.float32).astype(jnp.bfloat16)
        values = jnp.dot(block[0], value_up, preferred_element_type=jnp.float32).astype(
            jnp.bfloat16
        )
        return attend_block(state, q_heads, r_heads, k_nope, values, block[1])

    highest, total, weighted = over_blocks(
        start_state,
        (
            lax.all_gather(kv_latent, "sp", axis=0, tiled=True),
            lax.all_gather(rope_key, "sp", axis=0, tiled=True),
        ),
        latent_step,
    )
    attended = jnp.transpose((weighted / total[..., None]).astype(jnp.bfloat16), (1, 0, 2)).reshape(
        row_count, heads * value_size
    )
    glu = (row_scale * value_pre * jax.nn.sigmoid(row_scale * gate_pre)).astype(jnp.bfloat16)
    taps = conv_taps.shape[0]
    padded = padded_2(glu, (("sp", 0),), taps // 2).astype(jnp.float32)
    conv = jnp.zeros((row_count, local_ch), jnp.float32) + conv_bias
    for tap in range(taps):
        conv = conv + conv_taps[tap] * padded[tap : tap + row_count]
    channels = local_ch * lax.axis_size("tp")
    first_sum, second_sum = lax.psum((jnp.sum(conv, axis=-1), jnp.sum(conv * conv, axis=-1)), "tp")
    mean = first_sum[:, None] / channels
    spread = second_sum[:, None] / channels - mean * mean
    centred = conv - mean
    activated = jax.nn.silu(centred * lax.rsqrt(spread + eps_layer) * channel_gain).astype(
        jnp.bfloat16
    )
    contract = (((0,), (1,)), ((), ()))
    summed = lax.psum_scatter(
        (
            lax.dot_general(out_attend, attended, contract, preferred_element_type=jnp.float32)
            + lax.dot_general(out_conv, activated, contract, preferred_element_type=jnp.float32)
        ).astype(jnp.bfloat16),
        "tp",
        scatter_dimension=0,
        tiled=True,
    ).astype(jnp.float32)
    return jnp.transpose(summed).astype(jnp.bfloat16)


def solution(mesh):
    in_specs = (
        P("sp", "tp"),
        P(),
        P(),
        P(),
        P(),
        P(),
        P(),
        P(None, "tp"),
        P(None, "tp"),
        P(None, "tp"),
        P(None, "tp"),
        P(None, "tp"),
        P(None, "tp"),
        P(None, "tp"),
        P("tp"),
        P("tp"),
        P("tp", None),
        P("tp", None),
    )
    out_specs = P("sp", "tp")
    return jax.shard_map(
        per_device, mesh=mesh, in_specs=in_specs, out_specs=out_specs, check_vma=False
    )
```

profile of v0, /device:TPU:0, one launch (start us, length us, event | category | flops | bytes accessed | tf_op | source)
XLA Modules:
  0.0 147.2 jit_solution(18445132968032190985)
XLA Ops:
  8.5 1.6 %fusion.76 = (f32[1,512]{1,0:T(1,128)}, f32[1,512]{1,0:T(1,128)}, f32[1,512]{1,0:T(1,128)}, f32[1,512]{1,0:T(1,128)}, f32[1,512]{1,0:T(1,128)}, /*index=5*/f32[1...) fusion(f32[31,512]{1,0:T(8,128)} %param.33), kind=kLoop, calls=%fused_computation.139 | loop fusion | bytes 49152 | tf_op jit(solution)/shard_map/slice | solution.py:159
  10.1 1.8 %fusion.75 = (f32[1,512]{1,0:T(1,128)}, f32[1,512]{1,0:T(1,128)}, f32[1,512]{1,0:T(1,128)}, f32[1,512]{1,0:T(1,128)}, f32[1,512]{1,0:T(1,128)}, /*index=5*/f32[1...) fusion(f32[31,512]{1,0:T(8,128)} %param.33), kind=kLoop, calls=%fused_computation.138 | loop fusion | bytes 77824 | tf_op jit(solution)/shard_map/slice | solution.py:159
  12.0 16.4 %all-gather.3.cloned.1.call-done = bf16[256,2048]{1,0:T(8,128)(2,1)} async-done(((bf16[256,512]{1,0:T(8,128)(2,1)}), bf16[256,2048]{1,0:T(8,128)(2,1)}) %all-gather.3.cloned.1.call-update) | async-done | bytes 1048592 | tf_op jit(solution)/shard_map/all_gather | solution.py:102
  28.3 1.5 %fusion.21 = f32[256]{0:T(256)S(1)} fusion(bf16[256,2048]{1,0:T(8,128)(2,1)} %all-gather.3.cloned.1.call-done), kind=kLoop, calls=%fused_computation.29 | loop fusion | flops 1572608 | bytes 1049600 | tf_op jit(solution)/shard_map/reduce_sum | solution.py:108
  29.9 2.9 %fusion.26 = f32[256,512]{1,0:T(8,128)S(1)} fusion(bf16[2048,512]{1,0:T(8,128)(2,1)} %param.32, bf16[256,2048]{1,0:T(8,128)(2,1)} %all-gather.3.cloned.1.call-done, f32[2048]{0:T(1024)} %param.21, f32[256]{0:T(256)S(1)} %add_rsqrt_fusion.3), kind=kOutput, calls=%fused_computation.35 | convolution fusion | flops 538968064 | bytes 3679232 | tf_op jit(solution)/shard_map/dot_general | solution.py:106
  34.2 4.0 %collective-permute-start = (bf16[15,512]{1,0:T(8,128)(2,1)}, bf16[15,512]{1,0:T(8,128)(2,1)}, u32[]{:S(2)}, u32[]{:S(2)}) collective-permute-start(bf16[15,512]{1,0:T(8,128)(2,1)} %get-tuple-element.132), channel_id=1, source_target_pairs={{0,4},{4,8},{8,12},{12,16},{16,20},{20,24},{24,28},{1,5},{5,9},{9,... | collective-permute-start | bytes 46088 | tf_op jit(solution)/shard_map/ppermute | solution.py:20
  38.1 1.4 collective-permute-start.1
  39.6 0.8 multiply_reduce_fusion.1
  41.9 1.7 %convolution_multiply_fusion.4 = f32[256,32]{0,1:T(8,128)S(1)} fusion(bf16[2048,32]{0,1:T(8,128)(2,1)} %param.24, bf16[256,2048]{1,0:T(8,128)(2,1)} %all-gather.3.cloned.1.call-done, f32[2048]{0:T(1024)} %param.21, f32[256]{0:T(256)} %copy-done.41), kind=kOutput, calls=%fused_computation.42 | convolution fusion | flops 35135488 | bytes 1221632 | tf_op jit(solution)/shard_map/dot_general | solution.py:106
  43.9 0.8 multiply_cosine_fusion
  45.7 1.3 convolution_convert_fusion.2
  47.0 32.4 %all_gather.11 = bf16[2048,32]{0,1:T(8,128)(2,1)S(1)} all-gather(bf16[256,32]{0,1:T(8,128)(2,1)S(1)} %pad_maximum_fusion.1), channel_id=1, replica_groups=mesh['sp'=8,'tp'=4] {'sp'}, dimensions={0}, use_global_device_ids=true | all-gather | bytes 147456 | tf_op jit(solution)/shard_map/all_gather | solution.py:147
  80.1 0.8 maximum_convert_fusion
  81.2 3.3 %fusion.71 = (f32[256]{0:T(256)S(1)}, f32[256]{0:T(256)S(1)}, f32[256,512]{1,0:T(8,128)}) fusion(f32[286,512]{1,0:T(8,128)S(1)} %maximum_convert_fusion, f32[512]{0:T(512)S(1)} %bitcast.119, f32[512]{0:T(512)S(1)} %bitcast.120, f32[512]{0:T(512)S(1)} %bitcast.122, f32[512]{0:T(512)S(1)} %bitcast.123, f32[512]{0:T(512)S(1)} %bitcast.124, ...), kind=kLoop, calls=%fused_computation.135 | loop fusion | flops 8519168 | bytes 16844800 | tf_op jit(solution)/shard_map/reduce_sum | solution.py:161
  84.5 5.6 %all-reduce = (f32[256]{0:T(256)S(1)}, f32[256]{0:T(256)S(1)}) all-reduce(f32[256]{0:T(256)S(1)} %get-tuple-element.104, f32[256]{0:T(256)S(1)} %get-tuple-element.103), channel_id=1, replica_groups=mesh['sp'=8,'tp'=4] {'tp'}, use_global_device_ids=true, to_apply=%region_10.11 | all-reduce | flops 512 | bytes 4096 | tf_op jit(solution)/shard_map/psum | solution.py:161
  90.7 1.5 %copy.23 = bf16[2048,256]{1,0:T(8,128)(2,1)S(1)} copy(bf16[2048,256]{0,1:T(8,128)(2,1)} %all-gather.5.cloned.1.call-done) | data formatting | bytes 2097152
  92.2 19.9 %while.15 = (s32[]{:T(128)}, f32[4,256]{1,0:T(4,128)S(1)}, f32[4,256]{1,0:T(4,128)S(1)}, f32[4,256,64]{1,2,0:T(8,128)S(1)}, bf16[2,1024,256]{2,1,0:T(8,128)(2,1)...) while((s32[]{:T(128)}, f32[4,256]{1,0:T(4,128)S(1)}, ...), condition=%wide.region_6.7_spmd.clone, body=%wide.region_3.6_spmd.clone.sunk | while | flops 612045824 | bytes 42795232 | solution.py:74
  92.2 1.2 convolution_convert_fusion.5
  93.5 0.8 fusion.118
  94.4 2.7 %fusion.119 = (f32[4,256]{1,0:T(4,128)S(1)}, f32[4,256,1024]{1,2,0:T(8,128)}) fusion(bf16[256,4,32]{0,2,1:T(8,128)(2,1)S(1)} %copy-done.2, bf16[2,1024,32]{1,2,0:T(8,128)(2,1)S(1)} %copy-done.3, s32[]{:T(128)} %get-tuple-element.260, f32[4,1024,256]{2,1,0:T(8,128)S(1)} %fusion.118), kind=kOutput, calls=%fused_computation.136.clone.1 | convolution fusion | flops 70253568 | bytes 8523780 | tf_op jit(solution)/shard_map/while/body/eval_jaxpr/qhd,kd->hqk/dot_general | solution.py:54
  97.1 2.9 %fusion.120 = f32[4,256]{1,0:T(4,128)S(1)} fusion(f32[4,256,1024]{1,2,0:T(8,128)} %get-tuple-element.245, f32[4,256]{1,0:T(4,128)S(1)} %select_maximum_fusion.2), kind=kLoop, calls=%fused_computation.4.clone.1 | loop fusion | flops 2096128 | bytes 4202496 | tf_op jit(solution)/shard_map/while/body/eval_jaxpr/reduce_sum | solution.py:59
  100.0 1.3 convolution_convert_fusion.6
  101.3 0.8 fusion.122
  102.1 1.2 convolution_convert_fusion.5
  103.4 0.8 fusion.118
  104.3 2.7 %fusion.119 = (f32[4,256]{1,0:T(4,128)S(1)}, f32[4,256,1024]{1,2,0:T(8,128)}) fusion(bf16[256,4,32]{0,2,1:T(8,128)(2,1)S(1)} %copy-done.2, bf16[2,1024,32]{1,2,0:T(8,128)(2,1)S(1)} %copy-done.3, s32[]{:T(128)} %get-tuple-element.260, f32[4,1024,256]{2,1,0:T(8,128)S(1)} %fusion.118), kind=kOutput, calls=%fused_computation.136.clone.1 | convolution fusion | flops 70253568 | bytes 8523780 | tf_op jit(solution)/shard_map/while/body/eval_jaxpr/qhd,kd->hqk/dot_general | solution.py:54
  107.1 2.9 %fusion.120 = f32[4,256]{1,0:T(4,128)S(1)} fusion(f32[4,256,1024]{1,2,0:T(8,128)} %get-tuple-element.245, f32[4,256]{1,0:T(4,128)S(1)} %select_maximum_fusion.2), kind=kLoop, calls=%fused_computation.4.clone.1 | loop fusion | flops 2096128 | bytes 4202496 | tf_op jit(solution)/shard_map/while/body/eval_jaxpr/reduce_sum | solution.py:59
  110.0 1.2 convolution_convert_fusion.6
  111.3 0.8 fusion.122
  112.2 1.7 %fusion.78 = f32[256,2048]{1,0:T(8,128)S(1)} fusion(bf16[256,256]{0,1:T(8,128)(2,1)S(1)} %bitcast.106, bf16[256,2048]{1,0:T(8,128)(2,1)} %param.36), kind=kOutput, calls=%fused_computation.141 | convolution fusion | flops 268435456 | bytes 3276800 | tf_op jit(solution)/shard_map/dot_general | solution.py:171
  113.9 1.9 %fusion.20 = bf16[2048,256]{0,1:T(8,128)(2,1)} fusion(f32[256,2048]{1,0:T(8,128)S(1)} %fusion.78, bf16[512,2048]{1,0:T(8,128)(2,1)S(1)} %copy-done, f32[256,512]{1,0:T(8,128)S(1)} %copy-done.5, f32[512]{0:T(512)S(1)} %copy-done.47, f32[256]{0:T(256)S(1)} %copy-done.42, f32[256]{0:T(256)S(1)} %get-tuple-element.173), kind=kOutput, calls=%fused_computation.28 | convolution fusion | flops 538968064 | bytes 5771264 | tf_op jit(solution)/shard_map/dot_general | solution.py:172
  115.8 24.9 %reduce-scatter.2.cloned.1.call-done = bf16[512,256]{0,1:T(8,128)(2,1)} async-done(((bf16[2048,256]{0,1:T(8,128)(2,1)}), bf16[512,256]{0,1:T(8,128)(2,1)}) %reduce-scatter.2.cloned.1.call-update) | async-done | bytes 262160 | tf_op jit(solution)/shard_map/reduce_scatter | solution.py:169
  (136 shorter events, 7.6 us)
Async XLA Ops:
  6.5 107.4 %copy-start = (bf16[512,2048]{1,0:T(8,128)(2,1)S(1)}, bf16[512,2048]{1,0:T(8,128)(2,1)}, u32[]{:S(2)}) copy-start(bf16[512,2048]{1,0:T(8,128)(2,1)} %param.37) | copy-start | bytes 6291460
  6.5 21.8 %all-gather.3.cloned.1.call-start = ((), (), s32[]{:S(2)}) async-start(), calls=%async_computation.1 | async-start | bytes 1310720 | tf_op jit(solution)/shard_map/all_gather | solution.py:102
  7.3 83.4 %all-gather.5.cloned.1.call-start = ((), (), s32[]{:S(2)}) async-start(), calls=%async_computation.2 | async-start | bytes 1179648 | tf_op jit(solution)/shard_map/all_gather | solution.py:146
  34.2 45.9 %collective-permute-start = (bf16[15,512]{1,0:T(8,128)(2,1)}, bf16[15,512]{1,0:T(8,128)(2,1)}, u32[]{:S(2)}, u32[]{:S(2)}) collective-permute-start(bf16[15,512]{1,0:T(8,128)(2,1)} %get-tuple-element.132), channel_id=1, source_target_pairs={{0,4},{4,8},{8,12},{12,16},{16,20},{20,24},{24,28},{1,5},{5,9},{9,... | collective-permute-start | bytes 46088 | tf_op jit(solution)/shard_map/ppermute | solution.py:20
  38.1 41.9 %collective-permute-start.1 = (bf16[15,512]{1,0:T(8,128)(2,1)}, bf16[15,512]{1,0:T(8,128)(2,1)}, u32[]{:S(2)}, u32[]{:S(2)}) collective-permute-start(bf16[15,512]{1,0:T(8,128)(2,1)} %get-tuple-element.133), channel_id=1, source_target_pairs={{4,0},{8,4},{12,8},{16,12},{20,16},{24,20},{28,24},{5,1},{9,5},{13... | collective-permute-start | bytes 46088 | tf_op jit(solution)/shard_map/ppermute | solution.py:22
  41.8 98.9 %reduce-scatter.2.cloned.1.call-start = ((), (), s32[]{:S(2)}) async-start(), calls=%async_computation.3 | async-start | bytes 1310720 | tf_op jit(solution)/shard_map/reduce_scatter | solution.py:169
  43.6 37.3 %copy-start.8 = (f32[1,512]{1,0:T(1,128)S(1)}, f32[1,512]{1,0:T(1,128)}, u32[]{:S(2)}) copy-start(f32[1,512]{1,0:T(1,128)} %get-tuple-element.155) | copy-start | bytes 6148
  43.6 37.3 %copy-start.9 = (f32[1,512]{1,0:T(1,128)S(1)}, f32[1,512]{1,0:T(1,128)}, u32[]{:S(2)}) copy-start(f32[1,512]{1,0:T(1,128)} %get-tuple-element.156) | copy-start | bytes 6148
  43.6 37.3 %copy-start.10 = (f32[1,512]{1,0:T(1,128)S(1)}, f32[1,512]{1,0:T(1,128)}, u32[]{:S(2)}) copy-start(f32[1,512]{1,0:T(1,128)} %get-tuple-element.157) | copy-start | bytes 6148
  43.6 37.3 %copy-start.11 = (f32[1,512]{1,0:T(1,128)S(1)}, f32[1,512]{1,0:T(1,128)}, u32[]{:S(2)}) copy-start(f32[1,512]{1,0:T(1,128)} %get-tuple-element.158) | copy-start | bytes 6148
  43.6 37.3 %copy-start.12 = (f32[1,512]{1,0:T(1,128)S(1)}, f32[1,512]{1,0:T(1,128)}, u32[]{:S(2)}) copy-start(f32[1,512]{1,0:T(1,128)} %get-tuple-element.159) | copy-start | bytes 6148
  43.6 37.3 %copy-start.13 = (f32[1,512]{1,0:T(1,128)S(1)}, f32[1,512]{1,0:T(1,128)}, u32[]{:S(2)}) copy-start(f32[1,512]{1,0:T(1,128)} %get-tuple-element.160) | copy-start | bytes 6148
  43.6 37.3 %copy-start.14 = (f32[1,512]{1,0:T(1,128)S(1)}, f32[1,512]{1,0:T(1,128)}, u32[]{:S(2)}) copy-start(f32[1,512]{1,0:T(1,128)} %get-tuple-element.161) | copy-start | bytes 6148
  43.6 37.3 %copy-start.15 = (f32[1,512]{1,0:T(1,128)S(1)}, f32[1,512]{1,0:T(1,128)}, u32[]{:S(2)}) copy-start(f32[1,512]{1,0:T(1,128)} %get-tuple-element.162) | copy-start | bytes 6148
  43.6 37.3 %copy-start.16 = (f32[1,512]{1,0:T(1,128)S(1)}, f32[1,512]{1,0:T(1,128)}, u32[]{:S(2)}) copy-start(f32[1,512]{1,0:T(1,128)} %get-tuple-element.163) | copy-start | bytes 6148
  43.6 37.3 %copy-start.17 = (f32[1,512]{1,0:T(1,128)S(1)}, f32[1,512]{1,0:T(1,128)}, u32[]{:S(2)}) copy-start(f32[1,512]{1,0:T(1,128)} %get-tuple-element.164) | copy-start | bytes 6148
  43.7 37.3 %copy-start.18 = (f32[1,512]{1,0:T(1,128)S(1)}, f32[1,512]{1,0:T(1,128)}, u32[]{:S(2)}) copy-start(f32[1,512]{1,0:T(1,128)} %get-tuple-element.165) | copy-start | bytes 6148
  43.7 37.3 %copy-start.19 = (f32[1,512]{1,0:T(1,128)S(1)}, f32[1,512]{1,0:T(1,128)}, u32[]{:S(2)}) copy-start(f32[1,512]{1,0:T(1,128)} %get-tuple-element.166) | copy-start | bytes 6148
  43.7 37.3 %copy-start.20 = (f32[1,512]{1,0:T(1,128)S(1)}, f32[1,512]{1,0:T(1,128)}, u32[]{:S(2)}) copy-start(f32[1,512]{1,0:T(1,128)} %get-tuple-element.136) | copy-start | bytes 6148
  43.7 37.3 %copy-start.21 = (f32[1,512]{1,0:T(1,128)S(1)}, f32[1,512]{1,0:T(1,128)}, u32[]{:S(2)}) copy-start(f32[1,512]{1,0:T(1,128)} %get-tuple-element.137) | copy-start | bytes 6148
  43.7 37.3 %copy-start.22 = (f32[1,512]{1,0:T(1,128)S(1)}, f32[1,512]{1,0:T(1,128)}, u32[]{:S(2)}) copy-start(f32[1,512]{1,0:T(1,128)} %get-tuple-element.138) | copy-start | bytes 6148
  43.7 37.3 %copy-start.23 = (f32[1,512]{1,0:T(1,128)S(1)}, f32[1,512]{1,0:T(1,128)}, u32[]{:S(2)}) copy-start(f32[1,512]{1,0:T(1,128)} %get-tuple-element.139) | copy-start | bytes 6148
  43.7 37.3 %copy-start.24 = (f32[1,512]{1,0:T(1,128)S(1)}, f32[1,512]{1,0:T(1,128)}, u32[]{:S(2)}) copy-start(f32[1,512]{1,0:T(1,128)} %get-tuple-element.140) | copy-start | bytes 6148
  43.7 37.3 %copy-start.25 = (f32[1,512]{1,0:T(1,128)S(1)}, f32[1,512]{1,0:T(1,128)}, u32[]{:S(2)}) copy-start(f32[1,512]{1,0:T(1,128)} %get-tuple-element.141) | copy-start | bytes 6148
  43.7 37.3 %copy-start.26 = (f32[1,512]{1,0:T(1,128)S(1)}, f32[1,512]{1,0:T(1,128)}, u32[]{:S(2)}) copy-start(f32[1,512]{1,0:T(1,128)} %get-tuple-element.142) | copy-start | bytes 6148
  43.7 37.3 %copy-start.27 = (f32[1,512]{1,0:T(1,128)S(1)}, f32[1,512]{1,0:T(1,128)}, u32[]{:S(2)}) copy-start(f32[1,512]{1,0:T(1,128)} %get-tuple-element.143) | copy-start | bytes 6148
  43.8 37.3 %copy-start.28 = (f32[1,512]{1,0:T(1,128)S(1)}, f32[1,512]{1,0:T(1,128)}, u32[]{:S(2)}) copy-start(f32[1,512]{1,0:T(1,128)} %get-tuple-element.144) | copy-start | bytes 6148
  43.8 37.3 %copy-start.29 = (f32[1,512]{1,0:T(1,128)S(1)}, f32[1,512]{1,0:T(1,128)}, u32[]{:S(2)}) copy-start(f32[1,512]{1,0:T(1,128)} %get-tuple-element.145) | copy-start | bytes 6148
  43.8 37.3 %copy-start.30 = (f32[1,512]{1,0:T(1,128)S(1)}, f32[1,512]{1,0:T(1,128)}, u32[]{:S(2)}) copy-start(f32[1,512]{1,0:T(1,128)} %get-tuple-element.146) | copy-start | bytes 6148
  43.8 37.3 %copy-start.31 = (f32[1,512]{1,0:T(1,128)S(1)}, f32[1,512]{1,0:T(1,128)}, u32[]{:S(2)}) copy-start(f32[1,512]{1,0:T(1,128)} %get-tuple-element.147) | copy-start | bytes 6148
  43.8 37.3 %copy-start.32 = (f32[1,512]{1,0:T(1,128)S(1)}, f32[1,512]{1,0:T(1,128)}, u32[]{:S(2)}) copy-start(f32[1,512]{1,0:T(1,128)} %get-tuple-element.148) | copy-start | bytes 6148
  43.8 37.3 %copy-start.33 = (f32[1,512]{1,0:T(1,128)S(1)}, f32[1,512]{1,0:T(1,128)}, u32[]{:S(2)}) copy-start(f32[1,512]{1,0:T(1,128)} %get-tuple-element.149) | copy-start | bytes 6148
  (24 other events, 278.8 us)
Sparse Core Ops, SparseCore 0:
  8.9 19.4 all-gather.2
  42.0 40.8 all-gather.4
  116.0 24.6 reduce-scatter.1
where the time goes:
time: 148 us; the launch traced here: 147 us
  waiting for transfers between devices  42 us (28%)
  blocking collectives  38 us (26%)
  matrix products  25.4 us (17%)
  other arithmetic  15.5 us (10%)
  between operations  13.9 us (9%)
  local copies, waits for them, and re-layouts  6.72 us (5%)
  starting transfers between devices  5.47 us (4%)
    all_gather x1, blocking collectives, per_device(): lax.all_gather(rope_key, 'sp', axis=0, tiled=True)  32.4 us
    reduce_scatter x1, waiting for transfers between devices, per_device(): lax.psum_scatter((lax.dot_general(out_attend, attended, contract, preferr...  24.9 us
    all_gather x1, waiting for transfers between devices, per_device(): lax.all_gather(tokens, 'tp', axis=1, tiled=True).astype(jnp.float32)  16.4 us
    dot_general x5, matrix products, add_rows(): return jnp.dot(scaled, weight, preferred_element_type=jnp.float32)  6.63 us
    reduce_sum x2, other arithmetic, attend_block(): total = total * factor + jnp.sum(weight, axis=-1)  5.81 us
    psum x1, blocking collectives, per_device(): lax.psum((jnp.sum(conv, axis=-1), jnp.sum(conv * conv, axis=-1)), 'tp')  5.63 us
    dot_general x2, matrix products, attend_block(): jnp.einsum('qhd,kd->hqk', r_heads, rope_key, preferred_element_type=jnp.f...  5.41 us
    ppermute x1, starting transfers between devices, padded_2(): lax.ppermute(tail, axis, [(i, (i + 1) % count) for i in range(ends)])  3.98 us
  transfers between devices with their start and end apart: 5, of which 2 were waited for; matrix products, arithmetic and copies ran while one was open for 11% of the time, Pallas kernels for 0%

commit v1 on v0

--- a/solution.py
+++ b/solution.py
@@ -7,6 +7,19 @@
 eps_norm = 1e-06
 eps_layer = 1e-05
 theta = 10000.0
+
+
+def ring_gather(shard, axis, dim):
+    ways = lax.axis_size(axis)
+    up = [(d, (d + 1) % ways) for d in range(ways)]
+    down = [(d, (d - 1) % ways) for d in range(ways)]
+    earlier, later = ([shard], [shard])
+    for _ in range(ways // 2):
+        earlier.append(lax.ppermute(earlier[-1], axis, up))
+    for _ in range((ways - 1) // 2):
+        later.append(lax.ppermute(later[-1], axis, down))
+    line = jnp.concatenate([*earlier[::-1], *later[1:]], axis=dim)
+    return jnp.roll(line, (lax.axis_index(axis) - ways // 2) * shard.shape[dim], axis=dim)
 
 
 def padded_2(cells, sides, width):
@@ -99,7 +112,7 @@
     width = in_gain.shape[0]
     local_ch = conv_value.shape[1]
     positions = (lax.axis_index("sp") * row_count + jnp.arange(row_count)).astype(jnp.float32)
-    piece_f = lax.all_gather(tokens, "tp", axis=1, tiled=True).astype(jnp.float32)
+    piece_f = ring_gather(tokens, "tp", 1).astype(jnp.float32)
     scaled = (piece_f * in_gain).astype(jnp.bfloat16)
 
     def add_rows(weight):

time: 148 us -> 141 us (0.953)
  waiting for transfers between devices: 42 us -> 29.4 us
  starting transfers between devices: 5.47 us -> 12 us
  matrix products: 25.4 us -> 22.9 us
  local copies, waits for them, and re-layouts: 6.72 us -> 8.68 us
    all_gather x1 -> x0, waiting for transfers between devices: 16.4 us -> none  [per_device(): lax.all_gather(tokens, 'tp', axis=1, tiled=True).astype(jnp.float32)]
    ppermute x0 -> x3, starting transfers between devices: none -> 4.98 us  [the longest x2 3 us: ring_gather(): earlier.append(lax.ppermute(earlier[-1], axis, up))]
    dot_general x5, matrix products: 6.63 us -> 3.3 us  [add_rows(): return jnp.dot(scaled, weight, preferred_element_type=jnp.float32)]
    ppermute x0 -> x3, waiting for transfers between devices: none -> 3.17 us  [the longest x2 3.17 us: ring_gather(): earlier.append(lax.ppermute(earlier[-1], axis, up))]
    unnamed x91 -> x38, local copies, waits for them, and re-layouts: 1.69 us -> 3.63 us
    ppermute x1, starting transfers between devices: 3.98 us -> 5.58 us  [padded_2(): lax.ppermute(tail, axis, [(i, (i + 1) % count) for i in range(ends)])]
  transfers between devices with their start and end apart: 5 -> 7, of which waited for: 2 -> 3; matrix products, arithmetic and copies ran while one was open for 11% -> 13% of each run, Pallas kernels for 0% -> 0%
where the time goes in v1:
time: 141 us; the launch traced here: 140 us
  blocking collectives  38.6 us (27%)
  waiting for transfers between devices  29.4 us (21%)
  matrix products  22.9 us (16%)
  other arithmetic  14.6 us (10%)
  between operations  13.8 us (10%)
  starting transfers between devices  12 us (9%)
  local copies, waits for them, and re-layouts  8.68 us (6%)
    all_gather x1, blocking collectives, per_device(): lax.all_gather(rope_key, 'sp', axis=0, tiled=True)  32.9 us
    reduce_scatter x1, waiting for transfers between devices, per_device(): lax.psum_scatter((lax.dot_general(out_attend, attended, contract, preferr...  26.2 us
    reduce_sum x2, other arithmetic, attend_block(): total = total * factor + jnp.sum(weight, axis=-1)  5.81 us
    psum x1, blocking collectives, per_device(): lax.psum((jnp.sum(conv, axis=-1), jnp.sum(conv * conv, axis=-1)), 'tp')  5.76 us
    ppermute x1, starting transfers between devices, padded_2(): lax.ppermute(tail, axis, [(i, (i + 1) % count) for i in range(ends)])  5.58 us
    dot_general x2, matrix products, attend_block(): jnp.einsum('qhd,kd->hqk', r_heads, rope_key, preferred_element_type=jnp.f...  5.38 us
    reduce_sum x1, other arithmetic, per_device(): jnp.sum(conv, axis=-1)  4.27 us
    unnamed x38, local copies, waits for them, and re-layouts  3.63 us
  transfers between devices with their start and end apart: 7, of which 3 were waited for; matrix products, arithmetic and copies ran while one was open for 13% of the time, Pallas kernels for 0%

profile of v1, /device:TPU:0, one launch (start us, length us, event | category | flops | bytes accessed | tf_op | source)
XLA Modules:
  0.0 140.1 jit_solution(2870156354783790453)
XLA Ops:
  7.0 2.0 %collective-permute-start.2 = (bf16[256,512]{1,0:T(8,128)(2,1)}, bf16[256,512]{1,0:T(8,128)(2,1)S(1)}, u32[]{:S(2)}, u32[]{:S(2)}) collective-permute-start(bf16[256,512]{1,0:T(8,128)(2,1)} %param.20), channel_id=1, source_target_pairs={{0,3},{1,0},{2,1},{3,2},{4,7},{5,4},{6,5},{7,6},{8,11},{9,8},{10,9... | collective-permute-start | bytes 786440 | tf_op jit(solution)/shard_map/ppermute | solution.py:20
  9.6 1.6 %fusion.81 = (f32[1,512]{1,0:T(1,128)}, f32[1,512]{1,0:T(1,128)}, f32[1,512]{1,0:T(1,128)}, f32[1,512]{1,0:T(1,128)}, f32[1,512]{1,0:T(1,128)}, /*index=5*/f32[1...) fusion(f32[31,512]{1,0:T(8,128)} %param.33), kind=kLoop, calls=%fused_computation.152 | loop fusion | bytes 49152 | tf_op jit(solution)/shard_map/slice | solution.py:172
  11.2 2.3 %collective-permute-done = bf16[256,512]{1,0:T(8,128)(2,1)S(1)} collective-permute-done((bf16[256,512]{1,0:T(8,128)(2,1)}, bf16[256,512]{1,0:T(8,128)(2,1)S(1)}, u32[]{:S(2)}, u32[]{:S(2)}) %collective-permute-start) | collective-permute-done | bytes 262176 | tf_op jit(solution)/shard_map/ppermute | solution.py:18
  13.5 2.5 %collective-permute-start.1 = (bf16[256,512]{1,0:T(8,128)(2,1)S(1)}, bf16[256,512]{1,0:T(8,128)(2,1)S(1)}, u32[]{:S(2)}, u32[]{:S(2)}) collective-permute-start(bf16[256,512]{1,0:T(8,128)(2,1)S(1)} %collective-permute-done), channel_id=1, source_target_pairs={{0,1},{1,2},{2,3},{3,0},{4,5},{5,6},{6,7},{7,4},{8,9},{9,10},{10,1... | collective-permute-start | bytes 786440 | tf_op jit(solution)/shard_map/ppermute | solution.py:18
  16.6 1.8 %fusion.80 = (f32[1,512]{1,0:T(1,128)}, f32[1,512]{1,0:T(1,128)}, f32[1,512]{1,0:T(1,128)}, f32[1,512]{1,0:T(1,128)}, f32[1,512]{1,0:T(1,128)}, /*index=5*/f32[1...) fusion(f32[31,512]{1,0:T(8,128)} %param.33), kind=kLoop, calls=%fused_computation.151 | loop fusion | bytes 77824 | tf_op jit(solution)/shard_map/slice | solution.py:172
  18.4 0.9 collective-permute-done.1
  19.4 1.1 constant_dynamic-update-slice_fusion.5
  21.8 0.8 copy-done.12
  23.9 5.6 %collective-permute-start.3 = (bf16[15,512]{1,0:T(8,128)(2,1)}, bf16[15,512]{1,0:T(8,128)(2,1)}, u32[]{:S(2)}, u32[]{:S(2)}) collective-permute-start(bf16[15,512]{1,0:T(8,128)(2,1)} %get-tuple-element.132), channel_id=1, source_target_pairs={{0,4},{4,8},{8,12},{12,16},{16,20},{20,24},{24,28},{1,5},{5,9},{9,... | collective-permute-start | bytes 46088 | tf_op jit(solution)/shard_map/ppermute | solution.py:33
  29.5 1.4 %collective-permute-start.4 = (bf16[15,512]{1,0:T(8,128)(2,1)}, bf16[15,512]{1,0:T(8,128)(2,1)}, u32[]{:S(2)}, u32[]{:S(2)}) collective-permute-start(bf16[15,512]{1,0:T(8,128)(2,1)} %get-tuple-element.133), channel_id=1, source_target_pairs={{4,0},{8,4},{12,8},{16,12},{20,16},{24,20},{28,24},{5,1},{9,5},{13... | collective-permute-start | bytes 46088 | tf_op jit(solution)/shard_map/ppermute | solution.py:35
  30.9 0.8 multiply_reduce_fusion.1
  33.9 1.2 fusion.75
  35.7 1.3 convolution_convert_fusion.2
  37.0 32.9 %all_gather.7 = bf16[2048,32]{0,1:T(8,128)(2,1)S(1)} all-gather(bf16[256,32]{0,1:T(8,128)(2,1)S(1)} %pad_maximum_fusion.1), channel_id=1, replica_groups=mesh['sp'=8,'tp'=4] {'sp'}, dimensions={0}, use_global_device_ids=true | all-gather | bytes 147456 | tf_op jit(solution)/shard_map/all_gather | solution.py:160
  70.6 0.8 maximum_convert_fusion
  71.4 4.3 %fusion.76 = (f32[256]{0:T(256)S(1)}, f32[256]{0:T(256)S(1)}, f32[256,512]{1,0:T(8,128)}) fusion(f32[286,512]{1,0:T(8,128)S(1)} %maximum_convert_fusion, f32[512]{0:T(512)} %bitcast.119, f32[512]{0:T(512)} %bitcast.120, f32[512]{0:T(512)} %bitcast.122, f32[512]{0:T(512)} %bitcast.123, f32[512]{0:T(512)} %bitcast.124, f32[512]{0:T(512)} %bitcast.125, ...), kind=kLoop, calls=%fused_computation.148 | loop fusion | flops 8519168 | bytes 16844800 | tf_op jit(solution)/shard_map/reduce_sum | solution.py:174
  75.7 5.8 %all-reduce = (f32[256]{0:T(256)S(1)}, f32[256]{0:T(256)S(1)}) all-reduce(f32[256]{0:T(256)S(1)} %get-tuple-element.104, f32[256]{0:T(256)S(1)} %get-tuple-element.103), channel_id=1, replica_groups=mesh['sp'=8,'tp'=4] {'tp'}, use_global_device_ids=true, to_apply=%region_10.11 | all-reduce | flops 512 | bytes 4096 | tf_op jit(solution)/shard_map/psum | solution.py:174
  82.0 1.5 %copy.23 = bf16[2048,256]{1,0:T(8,128)(2,1)S(1)} copy(bf16[2048,256]{0,1:T(8,128)(2,1)} %all-gather.2.cloned.1.call-done) | data formatting | bytes 2097152
  83.5 19.9 %while.15 = (s32[]{:T(128)}, f32[4,256]{1,0:T(4,128)S(1)}, f32[4,256]{1,0:T(4,128)S(1)}, f32[4,256,64]{1,2,0:T(8,128)S(1)}, bf16[2,1024,256]{2,1,0:T(8,128)(2,1)...) while((s32[]{:T(128)}, f32[4,256]{1,0:T(4,128)S(1)}, ...), condition=%wide.region_6.7_spmd.clone, body=%wide.region_3.6_spmd.clone.sunk | while | flops 612045824 | bytes 42795232 | solution.py:87
  83.5 1.2 convolution_convert_fusion.5
  85.7 2.7 %fusion.124 = (f32[4,256]{1,0:T(4,128)S(1)}, f32[4,256,1024]{1,2,0:T(8,128)}) fusion(bf16[256,4,32]{0,2,1:T(8,128)(2,1)S(1)} %copy-done.2, bf16[2,1024,32]{1,2,0:T(8,128)(2,1)S(1)} %copy-done.3, s32[]{:T(128)} %get-tuple-element.260, f32[4,1024,256]{2,1,0:T(8,128)S(1)} %fusion.123), kind=kOutput, calls=%fused_computation.149.clone.1 | convolution fusion | flops 70253568 | bytes 8523780 | tf_op jit(solution)/shard_map/while/body/eval_jaxpr/qhd,kd->hqk/dot_general | solution.py:67
  88.4 2.9 %fusion.125 = f32[4,256]{1,0:T(4,128)S(1)} fusion(f32[4,256,1024]{1,2,0:T(8,128)} %get-tuple-element.245, f32[4,256]{1,0:T(4,128)S(1)} %select_maximum_fusion.2), kind=kLoop, calls=%fused_computation.4.clone.1 | loop fusion | flops 2096128 | bytes 4202496 | tf_op jit(solution)/shard_map/while/body/eval_jaxpr/reduce_sum | solution.py:72
  91.3 1.3 convolution_convert_fusion.6
  92.6 0.8 fusion.127
  93.4 1.2 convolution_convert_fusion.5
  95.6 2.7 %fusion.124 = (f32[4,256]{1,0:T(4,128)S(1)}, f32[4,256,1024]{1,2,0:T(8,128)}) fusion(bf16[256,4,32]{0,2,1:T(8,128)(2,1)S(1)} %copy-done.2, bf16[2,1024,32]{1,2,0:T(8,128)(2,1)S(1)} %copy-done.3, s32[]{:T(128)} %get-tuple-element.260, f32[4,1024,256]{2,1,0:T(8,128)S(1)} %fusion.123), kind=kOutput, calls=%fused_computation.149.clone.1 | convolution fusion | flops 70253568 | bytes 8523780 | tf_op jit(solution)/shard_map/while/body/eval_jaxpr/qhd,kd->hqk/dot_general | solution.py:67
  98.3 2.9 %fusion.125 = f32[4,256]{1,0:T(4,128)S(1)} fusion(f32[4,256,1024]{1,2,0:T(8,128)} %get-tuple-element.245, f32[4,256]{1,0:T(4,128)S(1)} %select_maximum_fusion.2), kind=kLoop, calls=%fused_computation.4.clone.1 | loop fusion | flops 2096128 | bytes 4202496 | tf_op jit(solution)/shard_map/while/body/eval_jaxpr/reduce_sum | solution.py:72
  101.2 1.3 convolution_convert_fusion.6
  102.5 0.8 fusion.127
  103.4 1.7 %fusion.83 = f32[256,2048]{1,0:T(8,128)S(1)} fusion(bf16[256,256]{0,1:T(8,128)(2,1)S(1)} %bitcast.106, bf16[256,2048]{1,0:T(8,128)(2,1)} %param.36), kind=kOutput, calls=%fused_computation.154 | convolution fusion | flops 268435456 | bytes 3276800 | tf_op jit(solution)/shard_map/dot_general | solution.py:184
  105.2 1.9 %fusion.20 = bf16[2048,256]{0,1:T(8,128)(2,1)} fusion(f32[256,2048]{1,0:T(8,128)S(1)} %fusion.83, bf16[512,2048]{1,0:T(8,128)(2,1)S(1)} %copy-done, f32[256,512]{1,0:T(8,128)S(1)} %copy-done.5, f32[512]{0:T(512)S(1)} %copy-done.17, f32[256]{0:T(256)S(1)} %copy-done.8, f32[256]{0:T(256)S(1)} %get-tuple-element.173), kind=kOutput, calls=%fused_computation.28 | convolution fusion | flops 538968064 | bytes 5771264 | tf_op jit(solution)/shard_map/dot_general | solution.py:185
  107.1 26.2 %reduce-scatter.2.cloned.1.call-done = bf16[512,256]{0,1:T(8,128)(2,1)} async-done(((bf16[2048,256]{0,1:T(8,128)(2,1)}), bf16[512,256]{0,1:T(8,128)(2,1)}) %reduce-scatter.2.cloned.1.call-update) | async-done | bytes 262160 | tf_op jit(solution)/shard_map/reduce_scatter | solution.py:182
  (87 shorter events, 10.1 us)
Async XLA Ops:
  6.5 98.6 %copy-start = (bf16[512,2048]{1,0:T(8,128)(2,1)S(1)}, bf16[512,2048]{1,0:T(8,128)(2,1)}, u32[]{:S(2)}) copy-start(bf16[512,2048]{1,0:T(8,128)(2,1)} %param.37) | copy-start | bytes 6291460
  6.5 14.1 %copy-start.4 = (bf16[256,512]{1,0:T(8,128)(2,1)S(1)}, bf16[256,512]{1,0:T(8,128)(2,1)}, u32[]{:S(2)}) copy-start(bf16[256,512]{1,0:T(8,128)(2,1)} %param.20) | copy-start | bytes 786436
  6.5 75.5 %all-gather.2.cloned.1.call-start = ((), (), s32[]{:S(2)}) async-start(), calls=%async_computation.1 | async-start | bytes 1179648 | tf_op jit(solution)/shard_map/all_gather | solution.py:159
  6.5 6.9 %collective-permute-start = (bf16[256,512]{1,0:T(8,128)(2,1)}, bf16[256,512]{1,0:T(8,128)(2,1)S(1)}, u32[]{:S(2)}, u32[]{:S(2)}) collective-permute-start(bf16[256,512]{1,0:T(8,128)(2,1)} %param.20), channel_id=1, source_target_pairs={{0,1},{1,2},{2,3},{3,0},{4,5},{5,6},{6,7},{7,4},{8,9},{9,10},{10,1... | collective-permute-start | bytes 786440 | tf_op jit(solution)/shard_map/ppermute | solution.py:18
  7.0 13.5 %collective-permute-start.2 = (bf16[256,512]{1,0:T(8,128)(2,1)}, bf16[256,512]{1,0:T(8,128)(2,1)S(1)}, u32[]{:S(2)}, u32[]{:S(2)}) collective-permute-start(bf16[256,512]{1,0:T(8,128)(2,1)} %param.20), channel_id=1, source_target_pairs={{0,3},{1,0},{2,1},{3,2},{4,7},{5,4},{6,5},{7,6},{8,11},{9,8},{10,9... | collective-permute-start | bytes 786440 | tf_op jit(solution)/shard_map/ppermute | solution.py:20
  13.5 5.8 %collective-permute-start.1 = (bf16[256,512]{1,0:T(8,128)(2,1)S(1)}, bf16[256,512]{1,0:T(8,128)(2,1)S(1)}, u32[]{:S(2)}, u32[]{:S(2)}) collective-permute-start(bf16[256,512]{1,0:T(8,128)(2,1)S(1)} %collective-permute-done), channel_id=1, source_target_pairs={{0,1},{1,2},{2,3},{3,0},{4,5},{5,6},{6,7},{7,4},{8,9},{9,10},{10,1... | collective-permute-start | bytes 786440 | tf_op jit(solution)/shard_map/ppermute | solution.py:18
  19.3 1.7 %copy-start.11 = (bf16[2048,512]{1,0:T(8,128)(2,1)S(1)}, bf16[2048,512]{1,0:T(8,128)(2,1)}, u32[]{:S(2)}) copy-start(bf16[2048,512]{1,0:T(8,128)(2,1)} %param.32) | copy-start | bytes 6291460
  19.4 1.7 %copy-start.16 = (f32[2048]{0:T(1024)S(1)}, f32[2048]{0:T(1024)}, u32[]{:S(2)}) copy-start(f32[2048]{0:T(1024)} %param.21) | copy-start | bytes 24580
  21.0 1.6 %copy-start.12 = (bf16[2048,512]{1,0:T(8,128)(2,1)S(1)}, bf16[2048,512]{1,0:T(8,128)(2,1)}, u32[]{:S(2)}) copy-start(bf16[2048,512]{1,0:T(8,128)(2,1)} %param.31) | copy-start | bytes 6291460
  22.6 8.3 %copy-start.13 = (bf16[2048,512]{1,0:T(8,128)(2,1)S(1)}, bf16[2048,512]{1,0:T(8,128)(2,1)}, u32[]{:S(2)}) copy-start(bf16[2048,512]{1,0:T(8,128)(2,1)} %param.22) | copy-start | bytes 6291460
  23.9 46.6 %collective-permute-start.3 = (bf16[15,512]{1,0:T(8,128)(2,1)}, bf16[15,512]{1,0:T(8,128)(2,1)}, u32[]{:S(2)}, u32[]{:S(2)}) collective-permute-start(bf16[15,512]{1,0:T(8,128)(2,1)} %get-tuple-element.132), channel_id=1, source_target_pairs={{0,4},{4,8},{8,12},{12,16},{16,20},{20,24},{24,28},{1,5},{5,9},{9,... | collective-permute-start | bytes 46088 | tf_op jit(solution)/shard_map/ppermute | solution.py:33
  29.5 2.2 %copy-start.15 = (bf16[2048,32]{0,1:T(8,128)(2,1)S(1)}, bf16[2048,32]{0,1:T(8,128)(2,1)}, u32[]{:S(2)}) copy-start(bf16[2048,32]{0,1:T(8,128)(2,1)} %param.24) | copy-start | bytes 393220
  29.5 2.7 %copy-start.14 = (bf16[2048,256]{1,0:T(8,128)(2,1)S(1)}, bf16[2048,256]{1,0:T(8,128)(2,1)}, u32[]{:S(2)}) copy-start(bf16[2048,256]{1,0:T(8,128)(2,1)} %param.23) | copy-start | bytes 3145732
  29.5 41.1 %collective-permute-start.4 = (bf16[15,512]{1,0:T(8,128)(2,1)}, bf16[15,512]{1,0:T(8,128)(2,1)}, u32[]{:S(2)}, u32[]{:S(2)}) collective-permute-start(bf16[15,512]{1,0:T(8,128)(2,1)} %get-tuple-element.133), channel_id=1, source_target_pairs={{4,0},{8,4},{12,8},{16,12},{20,16},{24,20},{28,24},{5,1},{9,5},{13... | collective-permute-start | bytes 46088 | tf_op jit(solution)/shard_map/ppermute | solution.py:35
  31.7 1.1 copy-start.7
  31.8 1.9 %copy-start.9 = (f32[256]{0:T(256)S(1)}, f32[256]{0:T(256)}, u32[]{:S(2)}) copy-start(f32[256]{0:T(256)} %add_convert_fusion.2) | copy-start | bytes 3076
  31.8 1.9 %copy-start.10 = (f32[16]{0:T(128)S(1)}, f32[16]{0:T(128)}, u32[]{:S(2)}) copy-start(f32[16]{0:T(128)} %multiply_power_fusion) | copy-start | bytes 196
  31.8 2.1 %copy-start.6 = (f32[512]{0:T(512)S(1)}, f32[512]{0:T(512)}, u32[]{:S(2)}) copy-start(f32[512]{0:T(512)} %param.25) | copy-start | bytes 6148
  33.6 99.6 %reduce-scatter.2.cloned.1.call-start = ((), (), s32[]{:S(2)}) async-start(), calls=%async_computation.2 | async-start | bytes 1310720 | tf_op jit(solution)/shard_map/reduce_scatter | solution.py:182
  84.7 0.8 copy-start.2
  84.8 0.9 copy-start.3
  88.4 4.2 %copy-start.1 = (f32[4,256,1024]{1,2,0:T(8,128)S(1)}, f32[4,256,1024]{1,2,0:T(8,128)}, u32[]{:S(2)}) copy-start(f32[4,256,1024]{1,2,0:T(8,128)} %get-tuple-element.245) | copy-start | bytes 12582916 | tf_op jit(solution)/shard_map/while
  94.7 0.8 copy-start.2
  94.7 0.9 copy-start.3
  98.3 4.2 %copy-start.1 = (f32[4,256,1024]{1,2,0:T(8,128)S(1)}, f32[4,256,1024]{1,2,0:T(8,128)}, u32[]{:S(2)}) copy-start(f32[4,256,1024]{1,2,0:T(8,128)} %get-tuple-element.245) | copy-start | bytes 12582916 | tf_op jit(solution)/shard_map/while
  103.4 1.8 %copy-start.5 = (f32[256,512]{1,0:T(8,128)S(1)}, f32[256,512]{1,0:T(8,128)}, u32[]{:S(2)}) copy-start(f32[256,512]{1,0:T(8,128)} %get-tuple-element.129) | copy-start | bytes 1572868
  103.4 1.8 %copy-start.8 = (f32[256]{0:T(256)S(1)}, f32[256]{0:T(256)}, u32[]{:S(2)}) copy-start(f32[256]{0:T(256)} %get-tuple-element.174) | copy-start | bytes 3076
  103.4 1.8 %copy-start.17 = (f32[512]{0:T(512)S(1)}, f32[512]{0:T(512)}, u32[]{:S(2)}) copy-start(f32[512]{0:T(512)} %param.35) | copy-start | bytes 6148
Sparse Core Ops, SparseCore 0:
  33.8 43.8 all-gather.1
  107.2 26.0 reduce-scatter.1
